TPU v7x, 32 devices: a whole 2x2x4 slice. The times are simulated.
32 devices in a mesh: grp: 2 (over y), ep: 4 (over z), tp: 4 (over x, core).
Axes of the slice: x: 2, y: 2, z: 4, core: 2. Of those that a mesh axis runs over, the one named last changes fastest.
Arguments:
- mix_rows: bfloat16 [4096, 2048], P(('grp', 'ep', 'tp')), parts along dimension 0, may hold values from -6 to 6
- expert_rows: bfloat16 [4096, 2048], P(('grp', 'ep', 'tp')), parts along dimension 0, may hold values from -6 to 6
- mix_gain: float32 [2048], replicated, may hold values from 0.1 to 1.9
- ffn_gain: float32 [2048], replicated, may hold values from 0.1 to 1.9
- w_query: bfloat16 [2048, 512], P(None, 'tp'), may hold values from -0.125 to 0.125
- w_key: bfloat16 [2048, 512], P(None, 'tp'), may hold values from -0.125 to 0.125
- w_value: bfloat16 [2048, 1024], P(None, 'tp'), may hold values from -0.125 to 0.125
- w_lowrank: bfloat16 [2048, 32], replicated, may hold values from -0.125 to 0.125
- w_decay: bfloat16 [32, 512], replicated, may hold values from -1 to 1
- decay_bias: float32 [512], replicated, may hold values from -1.5 to 16
- decay_shift: float32 [8, 4096], P('tp', ('grp', 'ep')), parts along dimension 1, may hold values from -2 to 0
- head_gain: float32 [128], replicated, may hold values from 0.1 to 1.9
- w_output: bfloat16 [1024, 2048], P('tp'), may hold values from -0.1875 to 0.1875
- route_ids: int32 [4096, 4], P(('grp', 'ep', 'tp')), parts along dimension 0, may hold values from 0 to 15, all different within a row; in each aligned block of 128 rows (0 to 127, 128 to 255, ...) at most 64 rows name the same one
- route_weights: float32 [4096, 4], P(('grp', 'ep', 'tp')), parts along dimension 0, may hold values from 0.3 to 1.2
- w_gate: bfloat16 [16, 2048, 512], P(('ep', 'tp')), may hold values from -0.125 to 0.125
- w_lift: bfloat16 [16, 2048, 512], P(('ep', 'tp')), may hold values from -0.125 to 0.125
- w_drop: bfloat16 [16, 512, 2048], P(('ep', 'tp')), may hold values from -0.25 to 0.25
- shared_gate: bfloat16 [2048, 512], P(None, 'tp'), may hold values from -0.125 to 0.125
- shared_lift: bfloat16 [2048, 512], P(None, 'tp'), may hold values from -0.125 to 0.125
- shared_drop: bfloat16 [512, 2048], P('tp'), may hold values from -0.25 to 0.25
Outputs:
- mixed: bfloat16 [4096, 2048], P(('grp', 'ep', 'tp')), parts along dimension 0
- expert_out: bfloat16 [4096, 2048], P(('grp', 'ep', 'tp')), parts along dimension 0
There are 2 independent parts, one for each index of `grp`. A program takes and returns all parts, laid end to end along the dimension named above; an argument that names none is the same for every part. Nothing has to cross between parts.
Inputs may be any that keep to these rules, and one draw needn't show every extreme that they name: `route_ids`: each row names 4 different experts. In each aligned block of 128 rows (the rows of one device) no expert is named by more than 64 rows.
All inputs are finite; a program needn't handle non-finite values.
Results may differ from a plain program's by a relative error of at most 0.014.
Values may be sent and summed in bfloat16 or wider, within the bound.
A program may use at most 128 MiB of HBM per device.

v0:
```python
import jax
import jax.numpy as jnp
from jax import lax
from jax.sharding import PartitionSpec as P

DK = 64
DV = 128
BLOCK = 64
epsilon = 1e-05
gate_norm = 16.0
highest = lax.Precision.HIGHEST


def entering_2(value, axis, combine, identity):
    length, mine = (lax.axis_size(axis), lax.axis_index(axis))
    everything = jax.tree.map(
        lambda part, kind: lax.all_gather(part.astype(kind), axis),
        value,
        (jnp.bfloat16, jnp.bfloat16),
    )
    start = jax.tree.map(
        lambda part, zero: jnp.broadcast_to(jnp.asarray(zero, part.dtype), part.shape),
        value,
        identity,
    )

    def lap(k, before):
        reached = k < mine
        new = combine(
            before, jax.tree.map(lambda part, own: part[k].astype(own.dtype), everything, value)
        )
        return jax.tree.map(lambda a, b: jnp.where(reached, a, b), new, before)

    return lax.fori_loop(0, length, lap, start)


def layer_norm(source, gain):
    values = source.astype(jnp.float32)
    center = values - jnp.mean(values, axis=-1, keepdims=True)
    inverse = lax.rsqrt(jnp.mean(center * center, axis=-1, keepdims=True) + epsilon)
    return (center * inverse * gain).astype(jnp.bfloat16)


def stored(product):
    return lax.optimization_barrier(product.astype(jnp.bfloat16)).astype(jnp.float32)


def gla_blocks(queries, key_rows, value_rows, log_decay, state_init):
    length, heads_here, key_width = queries.shape
    value_width = value_rows.shape[-1]
    blocks = length // BLOCK
    query_blocks = queries.reshape(blocks, BLOCK, heads_here, key_width)
    key_blocks = key_rows.reshape(blocks, BLOCK, heads_here, key_width)
    value_blocks = value_rows.reshape(blocks, BLOCK, heads_here, value_width)
    within = jnp.cumsum(log_decay.reshape(blocks, BLOCK, heads_here, key_width), axis=1)
    block_total = within[:, -1]
    scaled_query = query_blocks * jnp.exp(within)
    scaled_key = key_blocks * jnp.exp(-within)
    causal = jnp.tril(jnp.ones((BLOCK, BLOCK), dtype=jnp.bool_))
    scores = jnp.einsum("nihd,njhd->nhij", scaled_query, scaled_key, precision=highest)
    scores = jnp.where(causal, scores, 0.0)
    inside = jnp.einsum("nhij,njhv->nihv", scores, value_blocks, precision=highest)
    block_added = jnp.einsum(
        "njhd,njhv->nhdv",
        key_blocks * jnp.exp(block_total[:, None] - within),
        value_blocks,
        precision=highest,
    )

    def advance(state, inputs):
        decay_sum, addition = inputs
        return (jnp.exp(decay_sum)[:, :, None] * state + addition, state)

    final_state, entering = lax.scan(advance, state_init, (block_total, block_added))
    inside = inside + jnp.einsum("nihd,nhdv->nihv", scaled_query, entering, precision=highest)
    before = jnp.cumsum(block_total, axis=0) - block_total
    carried_query = query_blocks * jnp.exp(within + before[:, None])
    return (
        inside.reshape(length, heads_here, value_width),
        final_state,
        carried_query.reshape(length, heads_here, key_width),
        jnp.sum(block_total, axis=0),
    )


def body(
    mix_rows,
    expert_rows,
    mix_gain,
    ffn_gain,
    w_query,
    w_key,
    w_value,
    w_lowrank,
    w_decay,
    decay_bias,
    decay_shift,
    head_gain,
    w_output,
    route_ids,
    route_weights,
    w_gate,
    w_lift,
    w_drop,
    shared_gate,
    shared_lift,
    shared_drop,
):
    mix_normed = layer_norm(mix_rows, mix_gain)
    local_heads = w_query.shape[1] // DK
    key_cols = local_heads * DK
    value_cols = w_value.shape[1]
    column = lax.axis_index("tp") * key_cols
    decay_cols = lax.dynamic_slice_in_dim(w_decay, column, key_cols, 1)
    bias_cols = lax.dynamic_slice_in_dim(decay_bias, column, key_cols, 0)
    shard_rows = lax.all_gather(mix_normed, "tp", axis=0, tiled=True)
    query_part = jnp.dot(shard_rows, w_query, preferred_element_type=jnp.float32)
    key_part = jnp.dot(shard_rows, w_key, preferred_element_type=jnp.float32)
    value_part = jnp.dot(shard_rows, w_value, preferred_element_type=jnp.float32)
    lowrank = jnp.dot(shard_rows, w_lowrank, preferred_element_type=jnp.float32).astype(
        jnp.bfloat16
    )
    logits = jnp.dot(lowrank, decay_cols, preferred_element_type=jnp.float32) + bias_cols
    projected = jnp.concatenate(
        [stored(query_part), stored(key_part), stored(value_part), logits], axis=1
    )
    span_rows = projected.shape[0]
    queries = projected[:, :key_cols].reshape(span_rows, local_heads, DK) * DK ** (-0.5)
    key_rows = projected[:, key_cols : 2 * key_cols].reshape(span_rows, local_heads, DK)
    value_rows = projected[:, 2 * key_cols : 2 * key_cols + value_cols].reshape(
        span_rows, local_heads, DV
    )
    log_decay = (
        jax.nn.log_sigmoid(projected[:, 2 * key_cols + value_cols :]).reshape(
            span_rows, local_heads, DK
        )
        / gate_norm
        + jnp.transpose(decay_shift)[:, :, None]
    )
    zero_state = jnp.zeros((local_heads, DK, DV), jnp.float32)
    inside, final_state, carried_query, decay_total = gla_blocks(
        queries, key_rows, value_rows, log_decay, zero_state
    )

    def chain(earlier, later):
        return (earlier[0] + later[0], jnp.exp(later[0])[:, :, None] * earlier[1] + later[1])

    carried = entering_2(
        (decay_total, final_state), "ep", chain, (jnp.zeros_like(decay_total), zero_state)
    )
    entering = carried[1]
    attended = inside + jnp.einsum("rhd,hdv->rhv", carried_query, entering, precision=highest)
    inverse = lax.rsqrt(jnp.mean(attended * attended, axis=-1, keepdims=True) + epsilon)
    head_rows = (
        (attended * inverse * head_gain).astype(jnp.bfloat16).reshape(span_rows, local_heads * DV)
    )
    mixed = lax.psum_scatter(
        jnp.dot(head_rows, w_output, preferred_element_type=jnp.float32).astype(jnp.bfloat16),
        "tp",
        scatter_dimension=0,
        tiled=True,
    )
    expert_normed = layer_norm(expert_rows, ffn_gain)
    shard_rows = lax.all_gather(expert_normed, "tp", axis=0, tiled=True)
    hidden = (
        jax.nn.silu(jnp.dot(shard_rows, shared_gate, preferred_element_type=jnp.float32))
        * jnp.dot(shard_rows, shared_lift, preferred_element_type=jnp.float32)
    ).astype(jnp.bfloat16)
    shared_sum = lax.psum_scatter(
        jnp.dot(hidden, shared_drop, preferred_element_type=jnp.float32).astype(jnp.bfloat16),
        "tp",
        scatter_dimension=0,
        tiled=True,
    ).astype(jnp.float32)
    own_tokens, top_count = route_ids.shape
    local_experts = w_gate.shape[0]
    experts = lax.axis_size("ep") * lax.axis_size("tp") * local_experts
    capacity = 2 * own_tokens * top_count // experts
    flat_routes = route_ids.reshape(-1)
    matches = (flat_routes[:, None] == jnp.arange(experts, dtype=jnp.int32)[None, :]).astype(
        jnp.int32
    )
    slot_rank = jnp.sum((jnp.cumsum(matches, axis=0) - 1) * matches, axis=1)
    slot_index = flat_routes * capacity + slot_rank
    token_index = jnp.arange(own_tokens * top_count, dtype=jnp.int32) // top_count
    slot_token = (
        jnp.full((experts * capacity,), own_tokens, jnp.int32).at[slot_index].set(token_index)
    )
    padded = jnp.concatenate(
        [expert_normed, jnp.zeros((1, expert_normed.shape[1]), jnp.bfloat16)], axis=0
    )
    outgoing = padded[slot_token].reshape(experts, capacity, -1)
    arrived = lax.all_to_all(outgoing, ("ep", "tp"), split_axis=0, concat_axis=0, tiled=True)
    arrived_shape = arrived.shape
    grouped = arrived.reshape(-1, local_experts, arrived_shape[-2], arrived_shape[-1])
    gate_part = jnp.einsum("sepd,edf->sepf", grouped, w_gate, preferred_element_type=jnp.float32)
    lift_part = jnp.einsum("sepd,edf->sepf", grouped, w_lift, preferred_element_type=jnp.float32)
    inner = (jax.nn.silu(gate_part) * lift_part).astype(jnp.bfloat16)
    result = jnp.einsum("sepf,efd->sepd", inner, w_drop, preferred_element_type=jnp.float32)
    returned = lax.all_to_all(
        result.astype(jnp.bfloat16).reshape(arrived_shape),
        ("ep", "tp"),
        split_axis=0,
        concat_axis=0,
        tiled=True,
    )
    results = returned.reshape(experts * capacity, -1)[slot_index].reshape(
        own_tokens, top_count, -1
    )
    combined = shared_sum + jnp.sum(route_weights[:, :, None] * results.astype(jnp.float32), axis=1)
    return (mixed, combined.astype(jnp.bfloat16))


def solution(mesh):
    return jax.shard_map(
        body,
        mesh=mesh,
        in_specs=(
            P(("grp", "ep", "tp"), None),
            P(("grp", "ep", "tp"), None),
            P(),
            P(),
            P(None, "tp"),
            P(None, "tp"),
            P(None, "tp"),
            P(),
            P(),
            P(),
            P("tp", ("grp", "ep")),
            P(),
            P("tp", None),
            P(("grp", "ep", "tp"), None),
            P(("grp", "ep", "tp"), None),
            P(("ep", "tp"), None, None),
            P(("ep", "tp"), None, None),
            P(("ep", "tp"), None, None),
            P(None, "tp"),
            P(None, "tp"),
            P("tp", None),
        ),
        out_specs=(P(("grp", "ep", "tp"), None), P(("grp", "ep", "tp"), None)),
        check_vma=False,
    )
```

profile of v0, /device:TPU:0, one launch (start us, length us, event | category | flops | bytes accessed | tf_op | source)
XLA Modules:
  0.0 297.1 jit_solution(844361430291442152)
XLA Ops:
  10.8 2.4 scatter_custom_fusion
  17.3 6.0 %gather_fusion = bf16[1024,2048]{1,0:T(8,128)(2,1)} fusion(bf16[129,2048]{1,0:T(8,128)(2,1)S(1)} %concatenate.3, s32[1024]{0:T(1024)S(1)} %fusion.54), kind=kCustom, calls=%fused_computation | custom fusion | bytes 8392704 | tf_op jit(solution)/shard_map/gather | solution.py:192
  23.3 7.6 %all-to-all-start = ((bf16[16,64,2048]{2,1,0:T(8,128)(2,1)}), bf16[16,64,2048]{2,1,0:T(8,128)(2,1)}, u32[]{:S(2)}, u32[]{:S(2)}) async-start(bf16[16,64,2048]{2,1,0:T(8,128)(2,1)} %bitcast.142), calls=%async_computation.2 | async-start | bytes 8388608 | tf_op jit(solution)/shard_map/all_to_all | solution.py:193
  34.4 42.4 %all-gather.6.cloned.1.call-done = bf16[512,2048]{1,0:T(8,128)(2,1)} async-done(((bf16[128,2048]{1,0:T(8,128)(2,1)}), bf16[512,2048]{1,0:T(8,128)(2,1)}) %all-gather.6.cloned.1.call-update) | async-done | bytes 2097168 | tf_op jit(solution)/shard_map/all_gather | solution.py:116
  76.8 2.7 fusion.38
  80.4 2.6 convolution_convert_fusion.5
  84.2 2.7 convolution_convert_fusion.4
  88.0 2.6 convolution_convert_fusion.3
  90.6 19.8 %all-gather.8.cloned.1.call-done = bf16[512,2048]{1,0:T(8,128)(2,1)} async-done(((bf16[128,2048]{1,0:T(8,128)(2,1)}), bf16[512,2048]{1,0:T(8,128)(2,1)}) %all-gather.8.cloned.1.call-update) | async-done | bytes 2097168 | tf_op jit(solution)/shard_map/all_gather | solution.py:164
  110.5 2.4 fusion.63
  112.8 5.5 %convolution_convert_fusion.1 = bf16[512,2048]{1,0:T(8,128)(2,1)} fusion(bf16[128,2048]{1,0:T(8,128)(2,1)} %param.45, bf16[512,2048]{1,0:T(8,128)(2,1)} %all-gather.8.cloned.1.call-done, bf16[2048,128]{1,0:T(8,128)(2,1)} %param.44, f32[512,128]{1,0:T(8,128)S(1)} %fusion.63), kind=kOutput, calls=%fused_computation.12 | convolution fusion | flops 538312704 | bytes 5505024 | tf_op jit(solution)/shard_map/dot_general | solution.py:170
  119.5 3.1 %exponential_multiply_fusion = (f32[8,64,2,64]{3,0,1,2:T(8,128)S(1)}, f32[8,64,2,64]{3,0,1,2:T(8,128)}, f32[8,64,2,64]{3,0,1,2:T(8,128)}, f32[8,64,2,64]{3,0,1,2:T(8,128)S(1)}) fusion(f32[8,64,2,64]{3,0,1,2:T(8,128)} %copy-done.3, f32[8,64,2,64]{3,2,1,0:T(2,128)} %reshape.186, f32[8,2,64]{2,0,1:T(8,128)S(1)} %get-tuple-element.272, ...), kind=kLoop, calls=%fused_computation.65 | loop fusion | flops 393216 | bytes 1843200 | tf_op jit(solution)/shard_map/mul | solution.py:65
  123.9 6.9 %fusion.3 = f32[16,64,512]{2,1,0:T(8,128)} fusion(bf16[16,64,2048]{2,1,0:T(8,128)(2,1)} %all-to-all-done, bf16[1,2048,512]{2,1,0:T(8,128)(2,1)} %param.41), kind=kOutput, calls=%fused_computation.17 | convolution fusion | flops 2147483648 | bytes 8388608 | tf_op jit(solution)/shard_map/sepd,edf->sepf/dot_general | solution.py:197
  130.8 10.5 %convolution_convert_fusion = bf16[16,64,2048]{2,1,0:T(8,128)(2,1)} fusion(bf16[1,512,2048]{2,1,0:T(8,128)(2,1)S(1)} %copy-done, f32[16,64,512]{2,1,0:T(8,128)} %fusion.3, bf16[16,64,2048]{2,1,0:T(8,128)(2,1)} %all-to-all-done, bf16[1,2048,512]{2,1,0:T(8,128)(2,1)} %param.40), kind=kOutput, calls=%fused_computation.11 | convolution fusion | flops 4300210176 | bytes 14680064 | tf_op jit(solution)/shard_map/sepf,efd->sepd/dot_general | solution.py:199
  141.3 4.5 %all-to-all-start.1 = ((bf16[16,64,2048]{2,1,0:T(8,128)(2,1)}), bf16[16,64,2048]{2,1,0:T(8,128)(2,1)}, u32[]{:S(2)}, u32[]{:S(2)}) async-start(bf16[16,64,2048]{2,1,0:T(8,128)(2,1)} %convolution_convert_fusion), calls=%async_computation.3 | async-start | bytes 8388608 | tf_op jit(solution)/shard_map/all_to_all | solution.py:200
  145.9 13.0 %while.27 = (s32[]{:T(128)}, f32[2,64,128]{2,1,0:T(8,128)S(1)}, f32[8,2,64,128]{3,2,1,0:T(8,128)}, f32[8,2,64]{2,0,1:T(8,128)S(1)}, f32[8,2,64,128]{3,2,1,0:T(8,128)}, /*index=5*/s32[]{:T(128)}, s32[]{:T(128)}) while((s32[]{:T(128)}, f32[2,64,128]{2,1,0:T(8,128)S(1)}, f32[8,2,64,128]{3,2,1,0:T(8,128)}, f32[8,2,64]{2,0,1:T(8,128)S(1)}, ...), condition=%wide.region_4.5_spmd.clone, body=%wide.region_3.4_spmd.clone.sunk | while | flops 65539 | bytes 330848 | solution.py:74
  160.4 2.1 convolution_select_fusion
  167.9 52.2 %all-gather.2 = bf16[4,2,64]{2,1,0:T(2,128)(2,1)S(1)} all-gather(bf16[1,2,64]{2,1,0:T(2,128)(2,1)S(1)} %bitcast.152), channel_id=2, replica_groups=mesh['grp'=2,'ep'=4,'tp'=4] {'ep'}, dimensions={0}, use_global_device_ids=true | all-gather | bytes 1280 | tf_op jit(solution)/shard_map/all_gather | solution.py:17
  220.2 34.7 %all-gather.1 = bf16[8,64,128]{2,1,0:T(8,128)(2,1)S(1)} all-gather(bf16[2,64,128]{2,1,0:T(8,128)(2,1)} %convert_element_type.114), channel_id=3, replica_groups=mesh['grp'=2,'ep'=4,'tp'=4] {'ep'}, dimensions={0}, use_global_device_ids=true | all-gather | bytes 163840 | tf_op jit(solution)/shard_map/all_gather | solution.py:17
  257.2 2.1 convolution_convert_fusion.2
  260.2 7.9 %gather_fusion.1 = bf16[512,2048]{1,0:T(8,128)(2,1)} fusion(bf16[1024,2048]{1,0:T(8,128)(2,1)} %bitcast.29, s32[1024]{0:T(1024)S(1)} %pad_clamp_fusion), kind=kCustom, calls=%fused_computation.1 | custom fusion | bytes 4196352 | tf_op jit(solution)/shard_map/gather | solution.py:207
  268.2 4.9 %reshape.187 = f32[128,4,2048]{2,1,0:T(4,128)} reshape(bf16[512,2048]{1,0:T(8,128)(2,1)} %gather_fusion.1) | data formatting | bytes 6291456 | tf_op jit(solution)/shard_map/convert_element_type | solution.py:210
  273.0 5.4 %multiply_reduce_fusion = f32[128,2048]{1,0:T(8,128)S(1)} fusion(f32[128,4,2048]{2,1,0:T(4,128)} %reshape.187, f32[128,4]{1,0:T(8,128)S(1)} %copy.70), kind=kLoop, calls=%fused_computation.10 | loop fusion | flops 1835008 | bytes 5244928 | tf_op jit(solution)/shard_map/reduce_sum | solution.py:210
  280.4 10.2 %reduce-scatter.3.cloned.1.call-done = bf16[128,2048]{1,0:T(8,128)(2,1)} async-done(((bf16[512,2048]{1,0:T(8,128)(2,1)}), bf16[128,2048]{1,0:T(8,128)(2,1)}) %reduce-scatter.3.cloned.1.call-update) | async-done | bytes 524304 | tf_op jit(solution)/shard_map/reduce_scatter | solution.py:157
  (136 shorter events, 41.8 us)
Async XLA Ops:
  7.2 123.7 %copy-start = (bf16[1,512,2048]{2,1,0:T(8,128)(2,1)S(1)}, bf16[1,512,2048]{2,1,0:T(8,128)(2,1)}, u32[]{:S(2)}) copy-start(bf16[1,512,2048]{2,1,0:T(8,128)(2,1)} %param.42) | copy-start | bytes 6291460
  17.2 6.1 %copy-start.2 = (bf16[128,2048]{1,0:T(8,128)(2,1)}, bf16[128,2048]{1,0:T(8,128)(2,1)S(1)}, u32[]{:S(2)}) copy-start(bf16[128,2048]{1,0:T(8,128)(2,1)S(1)} %fusion.25) | copy-start | bytes 1572868
  23.3 7.7 %copy-start.1 = (bf16[128,2048]{1,0:T(8,128)(2,1)S(1)}, bf16[128,2048]{1,0:T(8,128)(2,1)}, u32[]{:S(2)}) copy-start(bf16[128,2048]{1,0:T(8,128)(2,1)} %param.25) | copy-start | bytes 1572868
  23.3 8.1 %copy-start.8 = (f32[2048]{0:T(1024)S(1)}, f32[2048]{0:T(1024)}, u32[]{:S(2)}) copy-start(f32[2048]{0:T(1024)} %param.27) | copy-start | bytes 24580
  23.3 100.6 %all-to-all-start = ((bf16[16,64,2048]{2,1,0:T(8,128)(2,1)}), bf16[16,64,2048]{2,1,0:T(8,128)(2,1)}, u32[]{:S(2)}, u32[]{:S(2)}) async-start(bf16[16,64,2048]{2,1,0:T(8,128)(2,1)} %bitcast.142), calls=%async_computation.2 | async-start | bytes 8388608 | tf_op jit(solution)/shard_map/all_to_all | solution.py:193
  30.9 2.6 copy-start.9
  30.9 45.9 %copy-start.12 = (bf16[2048,32]{0,1:T(8,128)(2,1)S(1)}, bf16[2048,32]{0,1:T(8,128)(2,1)}, u32[]{:S(2)}) copy-start(bf16[2048,32]{0,1:T(8,128)(2,1)} %param.32) | copy-start | bytes 393220
  30.9 45.9 %all-gather.6.cloned.1.call-start = ((), (), s32[]{:S(2)}) async-start(), calls=%async_computation.4 | async-start | bytes 2621440 | tf_op jit(solution)/shard_map/all_gather | solution.py:116
  32.6 77.8 %all-gather.8.cloned.1.call-start = ((), (), s32[]{:S(2)}) async-start(), calls=%async_computation.6 | async-start | bytes 2621440 | tf_op jit(solution)/shard_map/all_gather | solution.py:164
  33.4 245.0 %reduce-scatter.5.cloned.1.call-start = ((), (), s32[]{:S(2)}) async-start(), calls=%async_computation.7 | async-start | bytes 2621440 | tf_op jit(solution)/shard_map/reduce_scatter | solution.py:169
  80.4 6.4 %copy-start.3 = (f32[8,64,2,64]{3,0,1,2:T(8,128)}, f32[8,64,2,64]{3,0,1,2:T(8,128)S(1)}, u32[]{:S(2)}) copy-start(f32[8,64,2,64]{3,0,1,2:T(8,128)S(1)} %fusion.34) | copy-start | bytes 786436
  118.3 0.7 slice-start
  118.3 1.1 copy-start.4
  141.3 118.9 %all-to-all-start.1 = ((bf16[16,64,2048]{2,1,0:T(8,128)(2,1)}), bf16[16,64,2048]{2,1,0:T(8,128)(2,1)}, u32[]{:S(2)}, u32[]{:S(2)}) async-start(bf16[16,64,2048]{2,1,0:T(8,128)(2,1)} %convolution_convert_fusion), calls=%async_computation.3 | async-start | bytes 8388608 | tf_op jit(solution)/shard_map/all_to_all | solution.py:200
  145.8 144.7 %reduce-scatter.3.cloned.1.call-start = ((), (), s32[]{:S(2)}) async-start(), calls=%async_computation.5 | async-start | bytes 2621440 | tf_op jit(solution)/shard_map/reduce_scatter | solution.py:157
  159.8 3.1 %copy-start.7 = (f32[8,2,64,128]{3,2,1,0:T(8,128)S(1)}, f32[8,2,64,128]{3,2,1,0:T(8,128)}, u32[]{:S(2)}) copy-start(f32[8,2,64,128]{3,2,1,0:T(8,128)} %get-tuple-element.124) | copy-start | bytes 1572868
  162.9 2.8 copy-start.5
  165.7 91.4 %copy-start.11 = (f32[128]{0:T(128)S(1)}, f32[128]{0:T(128)}, u32[]{:S(2)}) copy-start(f32[128]{0:T(128)} %param.36) | copy-start | bytes 1540
  255.4 1.9 copy-start.6
  259.4 0.7 copy-start.10
Sparse Core Ops, SparseCore 0:
  33.8 42.9 all-gather.5
  78.4 32.0 all-gather.7
  118.5 29.2 reduce-scatter.4
  259.5 30.9 reduce-scatter.2
where the time goes:
time: 299 us; the launch traced here: 297 us
  blocking collectives  86.9 us (29%)
  waiting for transfers between devices  73.2 us (24%)
  matrix products  44.2 us (15%)
  local copies, waits for them, and re-layouts  33.6 us (11%)
  other arithmetic  32.3 us (11%)
  between operations  14.2 us (5%)
  starting transfers between devices  12.3 us (4%)
    all_gather x2, blocking collectives, entering_2(): lax.all_gather(part.astype(kind), axis)  86.9 us
    all_gather x1, waiting for transfers between devices, body(): shard_rows = lax.all_gather(mix_normed, 'tp', axis=0, tiled=True)  42.4 us
    all_gather x1, waiting for transfers between devices, body(): shard_rows = lax.all_gather(expert_normed, 'tp', axis=0, tiled=True)  19.8 us
    dot_general x1, matrix products, body(): jnp.einsum('sepf,efd->sepd', inner, w_drop, preferred_element_type=jnp.fl...  10.5 us
    reduce_scatter x1, waiting for transfers between devices, body(): lax.psum_scatter(jnp.dot(head_rows, w_output, preferred_element_type=jnp....  10.2 us
    gather x1, local copies, waits for them, and re-layouts, body(): returned.reshape(experts * capacity, -1)[slot_index]  7.94 us
    all_to_all x1, starting transfers between devices, body(): lax.all_to_all(outgoing, ('ep', 'tp'), split_axis=0, concat_axis=0, tiled...  7.58 us
    add x8, other arithmetic, advance(): return (jnp.exp(decay_sum)[:, :, None] * state + addition, state)  7.47 us
  transfers between devices with their start and end apart: 6, of which 3 were waited for; matrix products, arithmetic and copies ran while one was open for 31% of the time, Pallas kernels for 0%

commit v1 on v0

--- a/solution.py
+++ b/solution.py
@@ -161,7 +161,12 @@
         tiled=True,
     )
     expert_normed = layer_norm(expert_rows, ffn_gain)
-    shard_rows = lax.all_gather(expert_normed, "tp", axis=0, tiled=True)
+    ring = [expert_normed]
+    for hop in range(3):
+        ring.append(lax.ppermute(ring[-1], "tp", [(dev, (dev + 1) % 4) for dev in range(4)]))
+    shard_rows = jnp.roll(
+        jnp.concatenate(ring[::-1], axis=0), (lax.axis_index("tp") + 1) * ring[0].shape[0], axis=0
+    )
     hidden = (
         jax.nn.silu(jnp.dot(shard_rows, shared_gate, preferred_element_type=jnp.float32))
         * jnp.dot(shard_rows, shared_lift, preferred_element_type=jnp.float32)

time: 299 us -> 313 us (1.047)
  local copies, waits for them, and re-layouts: 33.6 us -> 41.9 us
  waiting for transfers between devices: 73.2 us -> 79.3 us
    ppermute x0 -> x3, waiting for transfers between devices: none -> 51.1 us  [body(): lax.ppermute(ring[-1], 'tp', [(dev, (dev + 1) % 4) for dev in range(4)])]
    all_gather x1, waiting for transfers between devices: 42.4 us -> 17.1 us  [body(): shard_rows = lax.all_gather(mix_normed, 'tp', axis=0, tiled=True)]
    all_gather x1 -> x0, waiting for transfers between devices: 19.8 us -> none  [body(): shard_rows = lax.all_gather(expert_normed, 'tp', axis=0, tiled=True)]
    unnamed x28 -> x42, local copies, waits for them, and re-layouts: 2.16 us -> 11.2 us
  transfers between devices with their start and end apart: 6 -> 8, of which waited for: 3 -> 5; matrix products, arithmetic and copies ran while one was open for 31% -> 32% of each run, Pallas kernels for 0% -> 0%
where the time goes in v1:
time: 313 us; the launch traced here: 311 us
  blocking collectives  86.5 us (28%)
  waiting for transfers between devices  79.3 us (25%)
  matrix products  44 us (14%)
  local copies, waits for them, and re-layouts  41.9 us (13%)
  other arithmetic  32.4 us (10%)
  between operations  14.3 us (5%)
  starting transfers between devices  12.6 us (4%)
    all_gather x2, blocking collectives, entering_2(): lax.all_gather(part.astype(kind), axis)  86.5 us
    ppermute x3, waiting for transfers between devices, body(): lax.ppermute(ring[-1], 'tp', [(dev, (dev + 1) % 4) for dev in range(4)])  51.1 us
    all_gather x1, waiting for transfers between devices, body(): shard_rows = lax.all_gather(mix_normed, 'tp', axis=0, tiled=True)  17.1 us
    unnamed x42, local copies, waits for them, and re-layouts  11.2 us
    reduce_scatter x1, waiting for transfers between devices, body(): lax.psum_scatter(jnp.dot(head_rows, w_output, preferred_element_type=jnp....  11 us
    dot_general x1, matrix products, body(): jnp.einsum('sepf,efd->sepd', inner, w_drop, preferred_element_type=jnp.fl...  10.1 us
    gather x1, local copies, waits for them, and re-layouts, body(): returned.reshape(experts * capacity, -1)[slot_index]  7.95 us
    all_to_all x1, starting transfers between devices, body(): lax.all_to_all(outgoing, ('ep', 'tp'), split_axis=0, concat_axis=0, tiled...  7.58 us
  transfers between devices with their start and end apart: 8, of which 5 were waited for; matrix products, arithmetic and copies ran while one was open for 32% of the time, Pallas kernels for 0%

profile of v1, /device:TPU:0, one launch (start us, length us, event | category | flops | bytes accessed | tf_op | source)
XLA Modules:
  0.0 311.2 jit_solution(9350790342577338965)
XLA Ops:
  13.3 2.4 scatter_custom_fusion
  18.1 6.0 %gather_fusion = bf16[1024,2048]{1,0:T(8,128)(2,1)} fusion(bf16[129,2048]{1,0:T(8,128)(2,1)S(1)} %concatenate.10, s32[1024]{0:T(1024)S(1)} %fusion.56), kind=kCustom, calls=%fused_computation | custom fusion | bytes 8392704 | tf_op jit(solution)/shard_map/gather | solution.py:197
  24.1 7.6 %all-to-all-start = ((bf16[16,64,2048]{2,1,0:T(8,128)(2,1)}), bf16[16,64,2048]{2,1,0:T(8,128)(2,1)}, u32[]{:S(2)}, u32[]{:S(2)}) async-start(bf16[16,64,2048]{2,1,0:T(8,128)(2,1)} %bitcast.140), calls=%async_computation.2 | async-start | bytes 8388608 | tf_op jit(solution)/shard_map/all_to_all | solution.py:198
  32.3 31.5 %collective-permute-done = bf16[128,2048]{1,0:T(8,128)(2,1)S(1)} collective-permute-done((bf16[128,2048]{1,0:T(8,128)(2,1)}, bf16[128,2048]{1,0:T(8,128)(2,1)S(1)}, u32[]{:S(2)}, u32[]{:S(2)}) %collective-permute-start) | collective-permute-done | bytes 524320 | tf_op jit(solution)/shard_map/ppermute | solution.py:166
  64.9 12.8 %collective-permute-done.1 = bf16[128,2048]{1,0:T(8,128)(2,1)} collective-permute-done((bf16[128,2048]{1,0:T(8,128)(2,1)S(1)}, bf16[128,2048]{1,0:T(8,128)(2,1)}, u32[]{:S(2)}, u32[]{:S(2)}) %collective-permute-start.1) | collective-permute-done | bytes 524320 | tf_op jit(solution)/shard_map/ppermute | solution.py:166
  80.0 6.8 %collective-permute-done.2 = bf16[128,2048]{1,0:T(8,128)(2,1)} collective-permute-done((bf16[128,2048]{1,0:T(8,128)(2,1)}, bf16[128,2048]{1,0:T(8,128)(2,1)}, u32[]{:S(2)}, u32[]{:S(2)}) %collective-permute-start.2) | collective-permute-done | bytes 524320 | tf_op jit(solution)/shard_map/ppermute | solution.py:166
  96.8 5.6 %convolution_convert_fusion.1 = bf16[512,2048]{1,0:T(8,128)(2,1)} fusion(bf16[128,2048]{1,0:T(8,128)(2,1)} %param.45, f32[512,128]{1,0:T(8,128)S(1)} %fusion.10, bf16[2048,128]{1,0:T(8,128)(2,1)} %param.43, bf16[1024,2048]{1,0:T(8,128)(2,1)} %copy-done.2, s32[]{:T(128)S(6)} %select_n.73), kind=kOutput, calls=%fused_computation.12 | convolution fusion | flops 538312704 | bytes 5505028 | tf_op jit(solution)/shard_map/dot_general | solution.py:175
  102.4 17.1 %all-gather.5.cloned.1.call-done = bf16[512,2048]{1,0:T(8,128)(2,1)} async-done(((bf16[128,2048]{1,0:T(8,128)(2,1)}), bf16[512,2048]{1,0:T(8,128)(2,1)}) %all-gather.5.cloned.1.call-update) | async-done | bytes 2097168 | tf_op jit(solution)/shard_map/all_gather | solution.py:116
  119.6 2.7 fusion.41
  123.2 2.6 convolution_convert_fusion.5
  126.9 2.6 convolution_convert_fusion.4
  130.6 2.6 convolution_convert_fusion.3
  133.3 3.1 exponential_multiply_fusion
  137.8 6.6 %fusion.3 = f32[16,64,512]{2,1,0:T(8,128)} fusion(bf16[16,64,2048]{2,1,0:T(8,128)(2,1)} %all-to-all-done, bf16[1,2048,512]{2,1,0:T(8,128)(2,1)} %param.41), kind=kOutput, calls=%fused_computation.17 | convolution fusion | flops 2147483648 | bytes 8388608 | tf_op jit(solution)/shard_map/sepd,edf->sepf/dot_general | solution.py:202
  144.4 10.1 %convolution_convert_fusion = bf16[16,64,2048]{2,1,0:T(8,128)(2,1)} fusion(bf16[1,512,2048]{2,1,0:T(8,128)(2,1)S(1)} %copy-done, f32[16,64,512]{2,1,0:T(8,128)} %fusion.3, bf16[16,64,2048]{2,1,0:T(8,128)(2,1)} %all-to-all-done, bf16[1,2048,512]{2,1,0:T(8,128)(2,1)} %param.40), kind=kOutput, calls=%fused_computation.11 | convolution fusion | flops 4300210176 | bytes 14680064 | tf_op jit(solution)/shard_map/sepf,efd->sepd/dot_general | solution.py:204
  154.5 4.5 %all-to-all-start.1 = ((bf16[16,64,2048]{2,1,0:T(8,128)(2,1)}), bf16[16,64,2048]{2,1,0:T(8,128)(2,1)}, u32[]{:S(2)}, u32[]{:S(2)}) async-start(bf16[16,64,2048]{2,1,0:T(8,128)(2,1)} %convolution_convert_fusion), calls=%async_computation.3 | async-start | bytes 8388608 | tf_op jit(solution)/shard_map/all_to_all | solution.py:205
  159.1 12.8 %while.27 = (s32[]{:T(128)}, f32[2,64,128]{2,1,0:T(8,128)S(1)}, f32[8,2,64,128]{3,2,1,0:T(8,128)}, f32[8,2,64]{2,0,1:T(8,128)S(1)}, f32[8,2,64,128]{3,2,1,0:T(8,128)}, /*index=5*/s32[]{:T(128)}, s32[]{:T(128)}) while((s32[]{:T(128)}, f32[2,64,128]{2,1,0:T(8,128)S(1)}, f32[8,2,64,128]{3,2,1,0:T(8,128)}, f32[8,2,64]{2,0,1:T(8,128)S(1)}, ...), condition=%wide.region_4.5_spmd.clone, body=%wide.region_3.4_spmd.clone.sunk | while | flops 65539 | bytes 330848 | solution.py:74
  181.4 52.0 %all-gather.2 = bf16[4,2,64]{2,1,0:T(2,128)(2,1)S(1)} all-gather(bf16[1,2,64]{2,1,0:T(2,128)(2,1)S(1)} %bitcast.150), channel_id=2, replica_groups=mesh['grp'=2,'ep'=4,'tp'=4] {'ep'}, dimensions={0}, use_global_device_ids=true | all-gather | bytes 1280 | tf_op jit(solution)/shard_map/all_gather | solution.py:17
  233.3 34.5 %all-gather.1 = bf16[8,64,128]{2,1,0:T(8,128)(2,1)S(1)} all-gather(bf16[2,64,128]{2,1,0:T(8,128)(2,1)S(1)} %convert_element_type.114), channel_id=3, replica_groups=mesh['grp'=2,'ep'=4,'tp'=4] {'ep'}, dimensions={0}, use_global_device_ids=true | all-gather | bytes 163840 | tf_op jit(solution)/shard_map/all_gather | solution.py:17
  270.1 3.4 %convolution_convert_fusion.2 = bf16[512,2048]{1,0:T(8,128)(2,1)} fusion(bf16[512,256]{0,1:T(8,128)(2,1)S(1)} %bitcast.142, bf16[256,2048]{1,0:T(8,128)(2,1)} %param.37), kind=kOutput, calls=%fused_computation.13 | convolution fusion | flops 537919488 | bytes 3407872 | tf_op jit(solution)/shard_map/dot_general | solution.py:158
  273.7 8.0 %gather_fusion.1 = bf16[512,2048]{1,0:T(8,128)(2,1)} fusion(bf16[1024,2048]{1,0:T(8,128)(2,1)} %bitcast.29, s32[1024]{0:T(1024)S(1)} %pad_clamp_fusion), kind=kCustom, calls=%fused_computation.1 | custom fusion | bytes 4196352 | tf_op jit(solution)/shard_map/gather | solution.py:212
  281.6 4.8 %reshape.187 = f32[128,4,2048]{2,1,0:T(4,128)} reshape(bf16[512,2048]{1,0:T(8,128)(2,1)} %gather_fusion.1) | data formatting | bytes 6291456 | tf_op jit(solution)/shard_map/convert_element_type | solution.py:215
  286.4 5.4 %multiply_reduce_fusion = f32[128,2048]{1,0:T(8,128)S(1)} fusion(f32[128,4,2048]{2,1,0:T(4,128)} %reshape.187, f32[128,4]{1,0:T(8,128)S(1)} %copy.70), kind=kLoop, calls=%fused_computation.10 | loop fusion | flops 1835008 | bytes 5244928 | tf_op jit(solution)/shard_map/reduce_sum | solution.py:215
  293.7 11.0 %reduce-scatter.3.cloned.1.call-done = bf16[128,2048]{1,0:T(8,128)(2,1)} async-done(((bf16[512,2048]{1,0:T(8,128)(2,1)}), bf16[128,2048]{1,0:T(8,128)(2,1)}) %reduce-scatter.3.cloned.1.call-update) | async-done | bytes 524304 | tf_op jit(solution)/shard_map/reduce_scatter | solution.py:157
  (154 shorter events, 53.8 us)
Async XLA Ops:
  7.2 137.2 %copy-start = (bf16[1,512,2048]{2,1,0:T(8,128)(2,1)S(1)}, bf16[1,512,2048]{2,1,0:T(8,128)(2,1)}, u32[]{:S(2)}) copy-start(bf16[1,512,2048]{2,1,0:T(8,128)(2,1)} %param.42) | copy-start | bytes 6291460
  13.3 2.5 copy-start.11
  17.2 0.8 copy-start.7
  24.1 8.1 %copy-start.3 = (bf16[128,2048]{1,0:T(8,128)(2,1)S(1)}, bf16[128,2048]{1,0:T(8,128)(2,1)}, u32[]{:S(2)}) copy-start(bf16[128,2048]{1,0:T(8,128)(2,1)} %param.25) | copy-start | bytes 1572868
  24.1 53.6 %copy-start.10 = (f32[2048]{0:T(1024)S(1)}, f32[2048]{0:T(1024)}, u32[]{:S(2)}) copy-start(f32[2048]{0:T(1024)} %param.27) | copy-start | bytes 24580
  24.1 54.9 %copy-start.13 = (f32[2,512]{1,0:T(2,128)S(1)}, f32[2,512]{1,0:T(2,128)}, u32[]{:S(2)}) copy-start(f32[2,512]{1,0:T(2,128)} %param.35) | copy-start | bytes 12292
  24.1 113.7 %all-to-all-start = ((bf16[16,64,2048]{2,1,0:T(8,128)(2,1)}), bf16[16,64,2048]{2,1,0:T(8,128)(2,1)}, u32[]{:S(2)}, u32[]{:S(2)}) async-start(bf16[16,64,2048]{2,1,0:T(8,128)(2,1)} %bitcast.140), calls=%async_computation.2 | async-start | bytes 8388608 | tf_op jit(solution)/shard_map/all_to_all | solution.py:198
  31.7 58.4 %copy-start.1 = (bf16[128,2048]{1,0:T(8,128)(2,1)S(1)}, bf16[128,2048]{1,0:T(8,128)(2,1)}, u32[]{:S(2)}) copy-start(bf16[128,2048]{1,0:T(8,128)(2,1)} %param.26) | copy-start | bytes 1572868
  31.7 58.4 %copy-start.9 = (f32[2048]{0:T(1024)S(1)}, f32[2048]{0:T(1024)}, u32[]{:S(2)}) copy-start(f32[2048]{0:T(1024)} %param.28) | copy-start | bytes 24580
  31.7 87.8 %all-gather.5.cloned.1.call-start = ((), (), s32[]{:S(2)}) async-start(), calls=%async_computation.4 | async-start | bytes 2621440 | tf_op jit(solution)/shard_map/all_gather | solution.py:116
  31.8 32.1 %collective-permute-start = (bf16[128,2048]{1,0:T(8,128)(2,1)}, bf16[128,2048]{1,0:T(8,128)(2,1)S(1)}, u32[]{:S(2)}, u32[]{:S(2)}) collective-permute-start(bf16[128,2048]{1,0:T(8,128)(2,1)} %copy-done.7), channel_id=1, source_target_pairs={{0,1},{1,2},{2,3},{3,0},{4,5},{5,6},{6,7},{7,4},{8,9},{9,10},{10,1... | collective-permute-start | bytes 1572872 | tf_op jit(solution)/shard_map/ppermute | solution.py:166
  64.6 13.1 %collective-permute-start.1 = (bf16[128,2048]{1,0:T(8,128)(2,1)S(1)}, bf16[128,2048]{1,0:T(8,128)(2,1)}, u32[]{:S(2)}, u32[]{:S(2)}) collective-permute-start(bf16[128,2048]{1,0:T(8,128)(2,1)S(1)} %collective-permute-done), channel_id=1, source_target_pairs={{0,1},{1,2},{2,3},{3,0},{4,5},{5,6},{6,7},{7,4},{8,9},{9,10},{10,1... | collective-permute-start | bytes 1572872 | tf_op jit(solution)/shard_map/ppermute | solution.py:166
  77.7 9.1 %collective-permute-start.2 = (bf16[128,2048]{1,0:T(8,128)(2,1)}, bf16[128,2048]{1,0:T(8,128)(2,1)}, u32[]{:S(2)}, u32[]{:S(2)}) collective-permute-start(bf16[128,2048]{1,0:T(8,128)(2,1)} %collective-permute-done.1), channel_id=1, source_target_pairs={{0,1},{1,2},{2,3},{3,0},{4,5},{5,6},{6,7},{7,4},{8,9},{9,10},{10,1... | collective-permute-start | bytes 1572872 | tf_op jit(solution)/shard_map/ppermute | solution.py:166
  78.9 212.9 %reduce-scatter.5.cloned.1.call-start = ((), (), s32[]{:S(2)}) async-start(), calls=%async_computation.6 | async-start | bytes 2621440 | tf_op jit(solution)/shard_map/reduce_scatter | solution.py:174
  80.0 16.2 %copy-start.8 = (bf16[2048,128]{1,0:T(8,128)(2,1)S(1)}, bf16[2048,128]{1,0:T(8,128)(2,1)}, u32[]{:S(2)}) copy-start(bf16[2048,128]{1,0:T(8,128)(2,1)} %param.44) | copy-start | bytes 1572868
  94.1 2.0 copy-start.2
  96.8 22.7 %copy-start.16 = (bf16[2048,32]{0,1:T(8,128)(2,1)S(1)}, bf16[2048,32]{0,1:T(8,128)(2,1)}, u32[]{:S(2)}) copy-start(bf16[2048,32]{0,1:T(8,128)(2,1)} %param.32) | copy-start | bytes 393220
  123.2 10.2 %copy-start.4 = (f32[8,64,2,64]{3,0,1,2:T(8,128)}, f32[8,64,2,64]{3,0,1,2:T(8,128)S(1)}, u32[]{:S(2)}) copy-start(f32[8,64,2,64]{3,0,1,2:T(8,128)S(1)} %fusion.37) | copy-start | bytes 786436
  154.5 119.2 %all-to-all-start.1 = ((bf16[16,64,2048]{2,1,0:T(8,128)(2,1)}), bf16[16,64,2048]{2,1,0:T(8,128)(2,1)}, u32[]{:S(2)}, u32[]{:S(2)}) async-start(bf16[16,64,2048]{2,1,0:T(8,128)(2,1)} %convolution_convert_fusion), calls=%async_computation.3 | async-start | bytes 8388608 | tf_op jit(solution)/shard_map/all_to_all | solution.py:205
  159.0 145.7 %reduce-scatter.3.cloned.1.call-start = ((), (), s32[]{:S(2)}) async-start(), calls=%async_computation.5 | async-start | bytes 2621440 | tf_op jit(solution)/shard_map/reduce_scatter | solution.py:157
  175.3 3.9 %copy-start.5 = (f32[8,64,2,64]{3,0,1,2:T(8,128)S(1)}, f32[8,64,2,64]{3,0,1,2:T(8,128)}, u32[]{:S(2)}) copy-start(f32[8,64,2,64]{3,0,1,2:T(8,128)} %get-tuple-element.200) | copy-start | bytes 786436
  175.3 94.8 %copy-start.15 = (f32[128]{0:T(128)S(1)}, f32[128]{0:T(128)}, u32[]{:S(2)}) copy-start(f32[128]{0:T(128)} %param.36) | copy-start | bytes 1540
  268.4 5.2 %copy-start.14 = (f32[128,4]{0,1:T(4,128)S(1)}, f32[128,4]{0,1:T(4,128)}, u32[]{:S(2)}) copy-start(f32[128,4]{0,1:T(4,128)} %param.39) | copy-start | bytes 6148
  268.4 5.3 %copy-start.12 = (s32[512,1]{0,1:T(1,128)S(1)}, s32[512,1]{0,1:T(1,128)}, u32[]{:S(2)}) copy-start(s32[512,1]{0,1:T(1,128)} %copy-done.11) | copy-start | bytes 6148
  (1 other events, 0.8 us)
Sparse Core Ops, SparseCore 0:
  79.0 40.5 all-gather.4
  122.1 30.2 reduce-scatter.4
  273.7 30.9 reduce-scatter.2
